TPU v7x, 32 devices: a whole 2x2x4 slice. The times are simulated.
32 devices in a mesh: ep: 8 (over z, x), tp: 4 (over y, core).
Axes of the slice: x: 2, y: 2, z: 4, core: 2. Of those that a mesh axis runs over, the one named last changes fastest.
Arguments:
- mixer_in: bfloat16 [1024, 2048], P('ep'), may hold values from -6 to 6
- mixer_gain: float32 [2048], replicated, may hold values from 0.1 to 1.9
- w_value: bfloat16 [2048, 1536], P(None, 'tp'), may hold values from -0.125 to 0.125
- w_gate: bfloat16 [2048, 1536], P(None, 'tp'), may hold values from -0.125 to 0.125
- w_taps: float32 [31, 1536], P(None, 'tp'), may hold values from -3 to 3
- channel_gain: float32 [1536], P('tp'), may hold values from 0.1 to 1.9
- w_output: bfloat16 [1536, 2048], P('tp'), may hold values from -0.15625 to 0.15625
- expert_in: bfloat16 [1024, 2048], P('ep'), may hold values from -6 to 6
- expert_gain: float32 [2048], replicated, may hold values from 0 to 8
- route_experts: int32 [1024, 4], P('ep'), may hold values from 0 to 7, all different within a row; in each aligned block of 128 rows (0 to 127, 128 to 255, ...) at most 128 rows name the same one
- route_scores: float32 [1024, 4], P('ep'), may hold values from -6 to 6
- expert_gate: bfloat16 [8, 2048, 2048], P('ep', None, 'tp'), may hold values from -0.125 to 0.125
- expert_up: bfloat16 [8, 2048, 2048], P('ep', None, 'tp'), may hold values from -0.125 to 0.125
- expert_down: bfloat16 [8, 2048, 2048], P('ep', 'tp'), may hold values from -0.125 to 0.125
Outputs:
- mixer_out: bfloat16 [1024, 2048], P('ep')
- expert_out: bfloat16 [1024, 2048], P('ep')
Inputs may be any that keep to these rules, and one draw needn't show every extreme that they name: `route_experts`: each row names 4 different experts. In each aligned block of 128 rows (the rows of one index of ep) no expert is named more than 128 times, a bound that some block reaches.
All inputs are finite; a program needn't handle non-finite values.
Results may differ from a plain program's by a relative error of at most 0.02.
Values may be sent and summed in bfloat16 or wider, within the bound.
A program may use at most 64 MiB of HBM per device.

v0:
```python
import jax
import jax.numpy as jnp
from jax import lax
from jax.sharding import PartitionSpec as P

CONV_CH = 1536
CONV_W = 31
TOP_K = 4
epsilon = 1e-05
clamp_limit = 7.0
swish_slope = 1.702


def shifted(block, axis, distance):
    devices = range(lax.axis_size(axis))
    route = [(i - distance, i) for i in devices if i - distance in devices]
    return lax.ppermute(block, axis, route)


def row_norm(inputs, gains):
    widened = inputs.astype(jnp.float32)
    row_mean = jnp.mean(widened, axis=-1, keepdims=True)
    row_var = jnp.mean(jnp.square(widened - row_mean), axis=-1, keepdims=True)
    return (widened - row_mean) * lax.rsqrt(row_var + epsilon) * gains


def local(
    mixer_in,
    mixer_gain,
    w_value,
    w_gate,
    w_taps,
    channel_gain,
    w_output,
    expert_in,
    expert_gain,
    route_experts,
    route_scores,
    expert_gate,
    expert_up,
    expert_down,
):
    normed = row_norm(mixer_in, mixer_gain).astype(jnp.bfloat16)
    values = jnp.dot(normed, w_value, preferred_element_type=jnp.float32)
    gate_pre = jnp.dot(normed, w_gate, preferred_element_type=jnp.float32)
    gated_values = (values * jax.nn.sigmoid(gate_pre)).astype(jnp.bfloat16)
    mixer_rows = gated_values.shape[0]
    reach_rows = CONV_W - 1
    earlier = shifted(gated_values[mixer_rows - reach_rows :], "ep", 1)
    extended = jnp.concatenate([earlier, gated_values], axis=0)
    conv_out = jnp.zeros(gated_values.shape, jnp.float32)
    for offset in range(CONV_W):
        conv_out = (
            conv_out + extended[offset : offset + mixer_rows].astype(jnp.float32) * w_taps[offset]
        )
    channel_sums = lax.psum(
        (
            jnp.sum(conv_out, axis=1, keepdims=True),
            jnp.sum(conv_out * conv_out, axis=1, keepdims=True),
        ),
        "tp",
    )
    row_mean = channel_sums[0] / CONV_CH
    row_var = channel_sums[1] / CONV_CH - row_mean * row_mean
    activated = jax.nn.silu(
        (conv_out - row_mean) * lax.rsqrt(row_var + epsilon) * channel_gain
    ).astype(jnp.bfloat16)
    mixer_out = lax.psum(
        jnp.dot(activated, w_output, preferred_element_type=jnp.float32).astype(jnp.bfloat16), "tp"
    )
    rows_b = expert_in.shape[0]
    width = expert_in.shape[1]
    experts = lax.axis_size("ep")
    capacity = 2 * rows_b * TOP_K // experts
    slot_share = capacity // lax.axis_size("tp")
    column = lax.axis_index("tp")
    normed_b = row_norm(expert_in, expert_gain).astype(jnp.bfloat16)
    raised = jnp.exp(route_scores)
    route_weights = raised / jnp.sum(raised, axis=1, keepdims=True)
    flat_ids = route_experts.reshape(-1)
    onehot = (flat_ids[:, None] == jnp.arange(experts, dtype=jnp.int32)[None, :]).astype(jnp.int32)
    slot_index = jnp.sum((jnp.cumsum(onehot, axis=0) - onehot) * onehot, axis=1)
    owner_row = jnp.arange(rows_b * TOP_K, dtype=jnp.int32) // TOP_K
    slot_table = (
        jnp.full((capacity * experts,), rows_b, jnp.int32)
        .at[slot_index * experts + flat_ids]
        .set(owner_row)
    )
    padded = jnp.concatenate([normed_b, jnp.zeros((1, width), jnp.bfloat16)], axis=0)
    gate_w = expert_gate[0]
    up_w = expert_up[0]
    down_w = expert_down[0]
    own_table = lax.dynamic_slice_in_dim(
        slot_table, column * slot_share * experts, slot_share * experts
    )
    sending = jnp.take(padded, own_table, axis=0).reshape(slot_share, experts, width)
    arrived = lax.all_to_all(sending, "ep", split_axis=1, concat_axis=1, tiled=True)
    block_rows = lax.all_gather(arrived, "tp", axis=0, tiled=True)
    flat_rows = block_rows.reshape(block_rows.shape[0] * block_rows.shape[1], block_rows.shape[2])
    gate_e = jnp.minimum(
        jnp.dot(flat_rows, gate_w, preferred_element_type=jnp.float32), clamp_limit
    )
    up_e = jnp.clip(
        jnp.dot(flat_rows, up_w, preferred_element_type=jnp.float32), -clamp_limit, clamp_limit
    )
    hidden = (
        ((up_e + 1.0) * gate_e * jax.nn.sigmoid(swish_slope * gate_e))
        .astype(jnp.bfloat16)
        .reshape(block_rows.shape[0], block_rows.shape[1], gate_w.shape[1])
        .reshape(capacity * experts, gate_w.shape[1])
    )
    summed = lax.psum_scatter(
        jnp.dot(hidden, down_w, preferred_element_type=jnp.float32).astype(jnp.bfloat16),
        "tp",
        scatter_dimension=0,
        tiled=True,
    )
    returned = lax.all_to_all(
        summed.reshape(slot_share, experts, width), "ep", split_axis=1, concat_axis=1, tiled=True
    )
    every_slot = lax.all_gather(returned, "tp", axis=0, tiled=True).reshape(
        capacity * experts, width
    )
    picked = jnp.take(every_slot, slot_index * experts + flat_ids, axis=0)
    picked = picked.reshape(rows_b, TOP_K, width).astype(jnp.float32)
    expert_out = jnp.sum(picked * route_weights[:, :, None], axis=1).astype(jnp.bfloat16)
    return (mixer_out, expert_out)


def solution(mesh):
    in_specs = (
        P("ep", None),
        P(),
        P(None, "tp"),
        P(None, "tp"),
        P(None, "tp"),
        P("tp"),
        P("tp", None),
        P("ep", None),
        P(),
        P("ep", None),
        P("ep", None),
        P("ep", None, "tp"),
        P("ep", None, "tp"),
        P("ep", "tp", None),
    )
    out_specs = (P("ep", None), P("ep", None))
    return jax.shard_map(local, mesh=mesh, in_specs=in_specs, out_specs=out_specs, check_vma=False)
```

profile of v0, /device:TPU:0, one launch (start us, length us, event | category | flops | bytes accessed | tf_op | source)
XLA Modules:
  0.0 263.1 jit_solution(18099323295168561547)
XLA Ops:
  7.2 0.0 copy-start
  7.2 0.0 all-gather.3.cloned.1.call-start
  7.2 0.9 copy.33
  8.2 0.1 eq.29
  8.3 0.1 eq.25
  8.4 0.1 reshape.119
  8.5 1.1 reduce-window.6
  9.7 0.2 slice_reduce_fusion
  9.9 0.1 fusion.68
  10.0 2.4 scatter_custom_fusion
  12.5 0.1 compare_and_fusion
  12.6 1.2 convert_reduce_fusion
  13.8 1.3 fusion.24
  15.1 0.1 broadcast_in_dim.49
  15.2 0.1 copy.38
  15.3 1.4 fusion.26
  16.8 2.3 gather_fusion
  19.1 2.4 copy_select_fusion
  21.6 32.8 %all_to_all.10 = bf16[32,8,2048]{2,0,1:T(8,128)(2,1)S(1)} all-to-all(bf16[32,8,2048]{2,0,1:T(8,128)(2,1)S(1)} %copy_select_fusion), channel_id=1, replica_groups=mesh['ep'=8,'tp'=4] {'ep'}, dimensions={1} | all-to-all | bytes 2097152 | tf_op jit(solution)/shard_map/all_to_all | solution.py:97
  54.4 1.6 copy.40
  56.0 0.0 all-gather.3.cloned.1.call-update
  56.0 0.0 reduce-scatter.2.cloned.1.call-start
  56.0 33.6 %all-gather.3.cloned.1.call-done = bf16[128,8,2048]{2,1,0:T(8,128)(2,1)} async-done(((bf16[32,8,2048]{2,1,0:T(8,128)(2,1)}), bf16[128,8,2048]{2,1,0:T(8,128)(2,1)}) %all-gather.3.cloned.1.call-update) | async-done | bytes 4194320 | tf_op jit(solution)/shard_map/all_gather | solution.py:98
  89.7 6.6 %fusion.2 = f32[1024,512]{1,0:T(8,128)} fusion(bf16[128,8,2048]{2,1,0:T(8,128)(2,1)} %all-gather.3.cloned.1.call-done, bf16[1,2048,512]{2,1,0:T(8,128)(2,1)} %param.26), kind=kOutput, calls=%fused_computation.5 | convolution fusion | flops 2147483648 | bytes 8388608 | tf_op jit(solution)/shard_map/dot_general | solution.py:104
  96.2 0.0 copy-done
  96.2 10.3 %convolution_convert_fusion = bf16[1024,2048]{1,0:T(8,128)(2,1)} fusion(bf16[1,512,2048]{2,1,0:T(8,128)(2,1)S(1)} %copy-done, f32[1024,512]{1,0:T(8,128)} %fusion.2, bf16[1,2048,512]{2,1,0:T(8,128)(2,1)} %param.25, bf16[128,8,2048]{2,1,0:T(8,128)(2,1)} %all-gather.3.cloned.1.call-done), kind=kOutput, calls=%fused_computation.8 | convolution fusion | flops 4302307328 | bytes 14680064 | tf_op jit(solution)/shard_map/dot_general | solution.py:113
  106.5 0.0 reduce-scatter.2.cloned.1.call-update
  106.6 0.0 all-gather.5.cloned.1.call-start
  106.6 44.7 %reduce-scatter.2.cloned.1.call-done = bf16[256,2048]{1,0:T(8,128)(2,1)} async-done(((bf16[1024,2048]{1,0:T(8,128)(2,1)}), bf16[256,2048]{1,0:T(8,128)(2,1)}) %reduce-scatter.2.cloned.1.call-update) | async-done | bytes 1048592 | tf_op jit(solution)/shard_map/reduce_scatter | solution.py:112
  151.3 1.8 copy.41
  153.1 30.9 %all_to_all.11 = bf16[32,8,2048]{2,0,1:T(8,128)(2,1)S(1)} all-to-all(bf16[32,8,2048]{2,0,1:T(8,128)(2,1)S(1)} %copy.41), channel_id=1, replica_groups=mesh['ep'=8,'tp'=4] {'ep'}, dimensions={1} | all-to-all | bytes 2097152 | tf_op jit(solution)/shard_map/all_to_all | solution.py:118
  184.0 1.6 copy.42
  185.6 0.0 all-gather.5.cloned.1.call-update
  185.6 0.2 all-reduce.4.cloned.1.call-start
  185.9 0.0 copy-start.5
  185.9 0.2 convert_reduce_fusion.1
  186.0 0.3 fusion.27
  186.3 1.9 fusion.81
  188.2 0.0 copy-done.5
  188.3 0.0 copy-start.4
  188.3 0.0 copy-start.2
  188.3 0.0 copy-start.3
  188.3 0.0 copy-start.7
  188.3 0.5 fusion.23
  188.9 3.4 %collective-permute-start = (bf16[30,384]{1,0:T(8,128)(2,1)S(1)}, bf16[30,384]{1,0:T(8,128)(2,1)S(1)}, u32[]{:S(2)}, u32[]{:S(2)}) collective-permute-start(bf16[30,384]{1,0:T(8,128)(2,1)S(1)} %slice.260), channel_id=1, source_target_pairs={{0,4},{4,8},{8,12},{12,16},{16,20},{20,24},{24,28},{1,5},{5,9},{9,... | collective-permute-start | bytes 69128 | tf_op jit(solution)/shard_map/ppermute | solution.py:17
  192.2 0.1 mul.528
  192.4 0.1 copy.35
  192.5 0.1 slice_reduce_fusion.30
  192.5 0.1 slice_reduce_fusion.31
  192.6 0.0 copy-done.3
  192.7 0.1 copy.36
  192.8 0.1 copy.43
  192.9 0.8 collective-permute-done
  193.7 0.9 fusion.83
  194.7 6.5 %all-reduce.1 = (f32[128,1]{0,1:T(1,128)S(1)}, f32[128,1]{0,1:T(1,128)S(1)}) all-reduce(f32[128,1]{0,1:T(1,128)S(1)} %bitcast.51, f32[128,1]{0,1:T(1,128)S(1)} %bitcast.50), channel_id=1, replica_groups=mesh['ep'=8,'tp'=4] {'tp'}, use_global_device_ids=true, to_apply=%region_5.0 | all-reduce | flops 256 | bytes 2048 | tf_op jit(solution)/shard_map/psum | solution.py:56
  201.1 0.0 copy-done.7
  201.1 2.7 %convolution_convert_fusion.1 = bf16[128,2048]{1,0:T(8,128)(2,1)} fusion(bf16[384,2048]{1,0:T(8,128)(2,1)} %param.20, f32[128,384]{1,0:T(8,128)S(1)} %get-tuple-element.39, f32[384]{0:T(512)S(1)} %copy-done.7, f32[128]{0:T(128)S(1)} %get-tuple-element.41, f32[128]{0:T(128)S(1)} %get-tuple-element.40), kind=kOutput, calls=%fused_computation.9 | convolution fusion | flops 201981952 | bytes 2296320 | tf_op jit(solution)/shard_map/dot_general | solution.py:69
  203.9 0.0 all-reduce.4.cloned.1.call-update
  203.9 14.5 %all-gather.5.cloned.1.call-done = bf16[128,8,2048]{2,1,0:T(8,128)(2,1)} async-done(((bf16[32,8,2048]{2,1,0:T(8,128)(2,1)}), bf16[128,8,2048]{2,1,0:T(8,128)(2,1)}) %all-gather.5.cloned.1.call-update) | async-done | bytes 4194320 | tf_op jit(solution)/shard_map/all_gather | solution.py:121
  218.4 8.0 %gather_fusion.1 = bf16[512,2048]{1,0:T(8,128)(2,1)} fusion(bf16[1024,2048]{1,0:T(8,128)(2,1)} %bitcast.44, s32[1024]{0:T(1024)S(1)} %pad_clamp_fusion), kind=kCustom, calls=%fused_computation.1 | custom fusion | bytes 4196352 | tf_op jit(solution)/shard_map/jit(_take)/gather | solution.py:124
  226.4 4.1 %gather.15 = bf16[128,4,2048]{2,1,0:T(4,128)(2,1)} reshape(bf16[512,2048]{1,0:T(8,128)(2,1)} %gather_fusion.1) | data formatting | bytes 4194304 | tf_op jit(solution)/shard_map/jit(_take)/gather | solution.py:124
  230.6 6.4 %multiply_reduce_fusion = bf16[128,2048]{1,0:T(8,128)(2,1)} fusion(f32[128,4]{1,0:T(8,128)S(1)} %copy.43, bf16[128,4,2048]{2,1,0:T(4,128)(2,1)} %gather.15, pred[128,4]{1,0:T(8,128)(4,1)S(1)} %copy.36), kind=kLoop, calls=%fused_computation.7 | loop fusion | flops 3932160 | bytes 2624000 | tf_op jit(solution)/shard_map/reduce_sum | solution.py:126
  237.0 17.7 %all-reduce.4.cloned.1.call-done = bf16[128,2048]{1,0:T(8,128)(2,1)} async-done(((bf16[128,2048]{1,0:T(8,128)(2,1)}), bf16[128,2048]{1,0:T(8,128)(2,1)}) %all-reduce.4.cloned.1.call-update) | async-done | bytes 524304 | tf_op jit(solution)/shard_map/psum | solution.py:68
  254.7 1.9 copy.46
  (24 shorter events, 0.2 us)
Async XLA Ops:
  7.2 89.1 %copy-start = (bf16[1,512,2048]{2,1,0:T(8,128)(2,1)S(1)}, bf16[1,512,2048]{2,1,0:T(8,128)(2,1)}, u32[]{:S(2)}) copy-start(bf16[1,512,2048]{2,1,0:T(8,128)(2,1)} %param.27) | copy-start | bytes 6291460
  7.2 82.5 %all-gather.3.cloned.1.call-start = ((), (), s32[]{:S(2)}) async-start(), calls=%async_computation.4 | async-start | bytes 5242880 | tf_op jit(solution)/shard_map/all_gather | solution.py:98
  56.0 95.3 %reduce-scatter.2.cloned.1.call-start = ((), (), s32[]{:S(2)}) async-start(), calls=%async_computation.5 | async-start | bytes 5242880 | tf_op jit(solution)/shard_map/reduce_scatter | solution.py:112
  106.6 111.9 %all-gather.5.cloned.1.call-start = ((), (), s32[]{:S(2)}) async-start(), calls=%async_computation.6 | async-start | bytes 5242880 | tf_op jit(solution)/shard_map/all_gather | solution.py:121
  184.0 1.8 copy-start.1
  184.0 2.3 copy-start.6
  185.6 69.1 %all-reduce.4.cloned.1.call-start = ((), (), s32[]{:S(2)}) async-start(), calls=%async_computation.3 | async-start | bytes 1048576 | tf_op jit(solution)/shard_map/psum | solution.py:68
  185.9 2.4 copy-start.5
  188.3 4.2 %copy-start.4 = (f32[128,4]{0,1:T(4,128)S(1)}, f32[128,4]{0,1:T(4,128)}, u32[]{:S(2)}) copy-start(f32[128,4]{0,1:T(4,128)} %param.24) | copy-start | bytes 6148
  188.3 4.2 %copy-start.2 = (f32[31,384]{1,0:T(8,128)S(1)}, f32[31,384]{1,0:T(8,128)}, u32[]{:S(2)}) copy-start(f32[31,384]{1,0:T(8,128)} %param.18) | copy-start | bytes 142852
  188.3 4.4 %copy-start.3 = (s32[128,4]{0,1:T(4,128)S(1)}, s32[128,4]{0,1:T(4,128)}, u32[]{:S(2)}) copy-start(s32[128,4]{0,1:T(4,128)} %param.23) | copy-start | bytes 6148
  188.3 12.9 %copy-start.7 = (f32[384]{0:T(512)S(1)}, f32[384]{0:T(512)}, u32[]{:S(2)}) copy-start(f32[384]{0:T(512)} %param.19) | copy-start | bytes 4612
  188.9 4.9 %collective-permute-start = (bf16[30,384]{1,0:T(8,128)(2,1)S(1)}, bf16[30,384]{1,0:T(8,128)(2,1)S(1)}, u32[]{:S(2)}, u32[]{:S(2)}) collective-permute-start(bf16[30,384]{1,0:T(8,128)(2,1)S(1)} %slice.260), channel_id=1, source_target_pairs={{0,4},{4,8},{8,12},{12,16},{16,20},{20,24},{24,28},{1,5},{5,9},{9,... | collective-permute-start | bytes 69128 | tf_op jit(solution)/shard_map/ppermute | solution.py:17
Sparse Core Ops, SparseCore 0:
  56.1 33.4 all-gather.2
  106.7 44.5 reduce-scatter.1
  185.7 32.6 all-gather.4
  221.2 33.4 all-reduce.3
where the time goes:
time: 264 us; the launch traced here: 263 us
  waiting for transfers between devices  111 us (42%)
  blocking collectives  70.2 us (27%)
  local copies, waits for them, and re-layouts  26 us (10%)
  matrix products  22.1 us (8%)
  other arithmetic  15.7 us (6%)
  between operations  14 us (5%)
  starting transfers between devices  3.71 us (1%)
    reduce_scatter x1, waiting for transfers between devices, local(): lax.psum_scatter(jnp.dot(hidden, down_w, preferred_element_type=jnp.float...  44.7 us
    all_gather x1, waiting for transfers between devices, local(): block_rows = lax.all_gather(arrived, 'tp', axis=0, tiled=True)  33.6 us
    all_to_all x1, blocking collectives, local(): lax.all_to_all(sending, 'ep', split_axis=1, concat_axis=1, tiled=True)  32.8 us
    all_to_all x1, blocking collectives, local(): lax.all_to_all(summed.reshape(slot_share, experts, width), 'ep', split_ax...  30.9 us
    psum x1, waiting for transfers between devices, local(): lax.psum(jnp.dot(activated, w_output, preferred_element_type=jnp.float32)...  17.7 us
    all_gather x1, waiting for transfers between devices, local(): lax.all_gather(returned, 'tp', axis=0, tiled=True)  14.5 us
    gather x2, local copies, waits for them, and re-layouts, local(): picked = jnp.take(every_slot, slot_index * experts + flat_ids, axis=0)  12.1 us
    dot_general x1, matrix products, local(): jnp.dot(hidden, down_w, preferred_element_type=jnp.float32)  10.3 us
  transfers between devices with their start and end apart: 5, of which 5 were waited for; matrix products, arithmetic and copies ran while one was open for 10% of the time, Pallas kernels for 0%

commit v1 on v0

--- a/solution.py
+++ b/solution.py
@@ -115,8 +115,18 @@
         scatter_dimension=0,
         tiled=True,
     )
-    returned = lax.all_to_all(
-        summed.reshape(slot_share, experts, width), "ep", split_axis=1, concat_axis=1, tiled=True
+    returned = jnp.concatenate(
+        jax.lax.all_to_all(
+            jnp.stack(
+                jnp.split(
+                    summed.reshape(slot_share, experts, width), jax.lax.axis_size("ep"), axis=1
+                )
+            ),
+            "ep",
+            0,
+            0,
+        ),
+        axis=1,
     )
     every_slot = lax.all_gather(returned, "tp", axis=0, tiled=True).reshape(
         capacity * experts, width

time: 264 us -> 268 us (1.015)
  local copies, waits for them, and re-layouts: 26 us -> 36.3 us
  waiting for transfers between devices: 111 us -> 105 us
    psum x1, waiting for transfers between devices: 17.7 us -> 11.1 us  [local(): lax.psum(jnp.dot(activated, w_output, preferred_element_type=jnp.float32)...]
    all_gather x0 -> x1, local copies, waits for them, and re-layouts: none -> 6.45 us  [local(): lax.all_gather(returned, 'tp', axis=0, tiled=True)]
    split x0 -> x1, local copies, waits for them, and re-layouts: none -> 6.37 us  [local(): jnp.split(summed.reshape(slot_share, experts, width), jax.lax.axis_size('...]
  transfers between devices with their start and end apart: 5 -> 5, of which waited for: 5 -> 5; matrix products, arithmetic and copies ran while one was open for 10% -> 12% of each run, Pallas kernels for 0% -> 0%
where the time goes in v1:
time: 268 us; the launch traced here: 267 us
  waiting for transfers between devices  105 us (39%)
  blocking collectives  70.4 us (26%)
  local copies, waits for them, and re-layouts  36.3 us (14%)
  matrix products  22.1 us (8%)
  other arithmetic  15.7 us (6%)
  between operations  14.1 us (5%)
  starting transfers between devices  3.71 us (1%)
    reduce_scatter x1, waiting for transfers between devices, local(): lax.psum_scatter(jnp.dot(hidden, down_w, preferred_element_type=jnp.float...  44.5 us
    all_gather x1, waiting for transfers between devices, local(): block_rows = lax.all_gather(arrived, 'tp', axis=0, tiled=True)  33.6 us
    all_to_all x1, blocking collectives, local(): lax.all_to_all(sending, 'ep', split_axis=1, concat_axis=1, tiled=True)  32.8 us
    all_to_all x1, blocking collectives, local(): jax.lax.all_to_all(jnp.stack(jnp.split(summed.reshape(slot_share, experts...  31 us
    all_gather x1, waiting for transfers between devices, local(): lax.all_gather(returned, 'tp', axis=0, tiled=True)  14.8 us
    gather x2, local copies, waits for them, and re-layouts, local(): picked = jnp.take(every_slot, slot_index * experts + flat_ids, axis=0)  12.2 us
    psum x1, waiting for transfers between devices, local(): lax.psum(jnp.dot(activated, w_output, preferred_element_type=jnp.float32)...  11.1 us
    dot_general x1, matrix products, local(): jnp.dot(hidden, down_w, preferred_element_type=jnp.float32)  10.3 us
  transfers between devices with their start and end apart: 5, of which 5 were waited for; matrix products, arithmetic and copies ran while one was open for 12% of the time, Pallas kernels for 0%

profile of v1, /device:TPU:0, one launch (start us, length us, event | category | flops | bytes accessed | tf_op | source)
XLA Modules:
  0.0 267.0 jit_solution(8943383415014041193)
XLA Ops:
  7.2 0.0 copy-start
  7.2 0.0 all-gather.4.cloned.1.call-start
  7.2 0.9 copy.57
  8.2 0.1 eq.29
  8.3 0.1 eq.25
  8.4 0.1 reshape.125
  8.5 1.1 reduce-window.6
  9.7 0.2 slice_reduce_fusion
  9.9 0.1 fusion.76
  10.0 2.4 scatter_custom_fusion
  12.5 0.1 compare_and_fusion
  12.6 1.2 convert_reduce_fusion
  13.8 1.3 fusion.24
  15.1 0.1 broadcast_in_dim.49
  15.2 0.1 copy.62
  15.3 1.4 fusion.26
  16.8 2.3 gather_fusion
  19.1 2.4 copy_select_fusion
  21.6 32.8 %all_to_all.10 = bf16[32,8,2048]{2,0,1:T(8,128)(2,1)S(1)} all-to-all(bf16[32,8,2048]{2,0,1:T(8,128)(2,1)S(1)} %copy_select_fusion), channel_id=1, replica_groups=mesh['ep'=8,'tp'=4] {'ep'}, dimensions={1} | all-to-all | bytes 2097152 | tf_op jit(solution)/shard_map/all_to_all | solution.py:97
  54.4 1.6 copy.64
  56.0 0.0 all-gather.4.cloned.1.call-update
  56.0 0.0 reduce-scatter.2.cloned.1.call-start
  56.0 33.6 %all-gather.4.cloned.1.call-done = bf16[128,8,2048]{2,1,0:T(8,128)(2,1)} async-done(((bf16[32,8,2048]{2,1,0:T(8,128)(2,1)}), bf16[128,8,2048]{2,1,0:T(8,128)(2,1)}) %all-gather.4.cloned.1.call-update) | async-done | bytes 4194320 | tf_op jit(solution)/shard_map/all_gather | solution.py:98
  89.7 6.6 %fusion.2 = f32[1024,512]{1,0:T(8,128)} fusion(bf16[128,8,2048]{2,1,0:T(8,128)(2,1)} %all-gather.4.cloned.1.call-done, bf16[1,2048,512]{2,1,0:T(8,128)(2,1)} %param.26), kind=kOutput, calls=%fused_computation.5 | convolution fusion | flops 2147483648 | bytes 8388608 | tf_op jit(solution)/shard_map/dot_general | solution.py:104
  96.2 10.3 %convolution_convert_fusion = bf16[1024,2048]{1,0:T(8,128)(2,1)} fusion(bf16[1,512,2048]{2,1,0:T(8,128)(2,1)S(1)} %copy-done, f32[1024,512]{1,0:T(8,128)} %fusion.2, bf16[1,2048,512]{2,1,0:T(8,128)(2,1)} %param.25, bf16[128,8,2048]{2,1,0:T(8,128)(2,1)} %all-gather.4.cloned.1.call-done), kind=kOutput, calls=%fused_computation.9 | convolution fusion | flops 4302307328 | bytes 14680064 | tf_op jit(solution)/shard_map/dot_general | solution.py:113
  106.5 0.0 reduce-scatter.2.cloned.1.call-update
  106.6 0.2 all-gather.6.cloned.1.call-start
  106.8 44.5 %reduce-scatter.2.cloned.1.call-done = bf16[256,2048]{1,0:T(8,128)(2,1)} async-done(((bf16[1024,2048]{1,0:T(8,128)(2,1)}), bf16[256,2048]{1,0:T(8,128)(2,1)}) %reduce-scatter.2.cloned.1.call-update) | async-done | bytes 1048592 | tf_op jit(solution)/shard_map/reduce_scatter | solution.py:112
  151.3 6.4 %fusion.92 = (bf16[32,1,2048]{2,1,0:T(2,128)(2,1)S(1)}, bf16[32,1,2048]{2,1,0:T(2,128)(2,1)S(1)}, bf16[32,1,2048]{2,1,0:T(2,128)(2,1)S(1)}, bf16[32,1,2048]{2,1,...) fusion(bf16[32,8,2048]{2,1,0:T(8,128)(2,1)} %bitcast.82), kind=kLoop, calls=%fused_computation.219 | loop fusion | bytes 2097152 | tf_op jit(solution)/shard_map/split | solution.py:121
  157.7 0.1 fusion.41
  157.8 0.1 fusion.40
  157.8 0.1 fusion.39
  157.9 0.1 fusion.38
  158.0 0.1 fusion.37
  158.1 0.1 fusion.36
  158.2 0.1 fusion.35
  158.3 0.1 fusion.34
  158.4 0.0 copy-start.6
  158.4 31.0 %all_to_all.11 = bf16[8,32,1,2048]{3,1,2,0:T(8,128)(2,1)} all-to-all(bf16[8,32,1,2048]{3,1,2,0:T(8,128)(2,1)S(1)} %fusion.34), channel_id=1, replica_groups=mesh['ep'=8,'tp'=4] {'ep'}, dimensions={0} | all-to-all | bytes 2097152 | tf_op jit(solution)/shard_map/all_to_all | solution.py:119
  189.4 0.0 all-gather.6.cloned.1.call-update
  189.5 0.0 all-reduce.4.cloned.1.call-start
  189.5 0.2 convert_reduce_fusion.1
  189.7 0.3 fusion.27
  190.0 1.9 fusion.89
  192.0 0.5 fusion.23
  192.5 3.4 %collective-permute-start = (bf16[30,384]{1,0:T(8,128)(2,1)S(1)}, bf16[30,384]{1,0:T(8,128)(2,1)S(1)}, u32[]{:S(2)}, u32[]{:S(2)}) collective-permute-start(bf16[30,384]{1,0:T(8,128)(2,1)S(1)} %slice.260), channel_id=1, source_target_pairs={{0,4},{4,8},{8,12},{12,16},{16,20},{20,24},{24,28},{1,5},{5,9},{9,... | collective-permute-start | bytes 69128 | tf_op jit(solution)/shard_map/ppermute | solution.py:17
  195.9 0.1 mul.528
  196.0 0.1 copy.59
  196.1 0.1 slice_reduce_fusion.30
  196.2 0.1 slice_reduce_fusion.31
  196.4 0.1 copy.60
  196.5 0.1 copy.74
  196.6 0.8 collective-permute-done
  197.4 0.9 fusion.91
  198.3 6.5 %all-reduce.1 = (f32[128,1]{0,1:T(1,128)S(1)}, f32[128,1]{0,1:T(1,128)S(1)}) all-reduce(f32[128,1]{0,1:T(1,128)S(1)} %bitcast.87, f32[128,1]{0,1:T(1,128)S(1)} %bitcast.86), channel_id=1, replica_groups=mesh['ep'=8,'tp'=4] {'tp'}, use_global_device_ids=true, to_apply=%region_5.0 | all-reduce | flops 256 | bytes 2048 | tf_op jit(solution)/shard_map/psum | solution.py:56
  204.8 2.7 %convolution_convert_fusion.1 = bf16[128,2048]{1,0:T(8,128)(2,1)} fusion(bf16[384,2048]{1,0:T(8,128)(2,1)} %param.20, f32[128,384]{1,0:T(8,128)S(1)} %get-tuple-element.39, f32[384]{0:T(512)S(1)} %copy-done.7, f32[128]{0:T(128)S(1)} %get-tuple-element.49, f32[128]{0:T(128)S(1)} %get-tuple-element.48), kind=kOutput, calls=%fused_computation.10 | convolution fusion | flops 201981952 | bytes 2296320 | tf_op jit(solution)/shard_map/dot_general | solution.py:69
  207.5 0.0 all-reduce.4.cloned.1.call-update
  207.6 14.8 %all-gather.6.cloned.1.call-done = bf16[128,8,1,2048]{3,0,2,1:T(8,128)(2,1)} async-done(((bf16[32,8,1,2048]{3,0,2,1:T(8,128)(2,1)}), bf16[128,8,1,2048]{3,0,2,1:T(8,128)(2,1)}) %all-gather.6.cloned.1.call-update) | async-done | bytes 4194320 | tf_op jit(solution)/shard_map/all_gather | solution.py:131
  222.4 6.5 %copy.109 = bf16[128,8,1,2048]{3,1,0,2:T(8,128)(2,1)} copy(bf16[128,8,1,2048]{3,0,2,1:T(8,128)(2,1)} %all-gather.6.cloned.1.call-done) | data formatting | bytes 8388608 | tf_op jit(solution)/shard_map/all_gather | solution.py:131
  228.8 8.1 %gather_fusion.1 = bf16[512,2048]{1,0:T(8,128)(2,1)} fusion(bf16[1024,2048]{1,0:T(8,128)(2,1)} %bitcast.79, s32[1024]{0:T(1024)S(1)} %pad_clamp_fusion), kind=kCustom, calls=%fused_computation.1 | custom fusion | bytes 4196352 | tf_op jit(solution)/shard_map/jit(_take)/gather | solution.py:134
  236.9 4.1 %gather.15 = bf16[128,4,2048]{2,1,0:T(4,128)(2,1)} reshape(bf16[512,2048]{1,0:T(8,128)(2,1)} %gather_fusion.1) | data formatting | bytes 4194304 | tf_op jit(solution)/shard_map/jit(_take)/gather | solution.py:134
  241.0 6.4 %multiply_reduce_fusion = bf16[128,2048]{1,0:T(8,128)(2,1)} fusion(f32[128,4]{1,0:T(8,128)S(1)} %copy.74, bf16[128,4,2048]{2,1,0:T(4,128)(2,1)} %gather.15, pred[128,4]{1,0:T(8,128)(4,1)S(1)} %copy.60), kind=kLoop, calls=%fused_computation.8 | loop fusion | flops 3932160 | bytes 2624000 | tf_op jit(solution)/shard_map/reduce_sum | solution.py:136
  247.5 11.1 %all-reduce.4.cloned.1.call-done = bf16[128,2048]{1,0:T(8,128)(2,1)} async-done(((bf16[128,2048]{1,0:T(8,128)(2,1)}), bf16[128,2048]{1,0:T(8,128)(2,1)}) %all-reduce.4.cloned.1.call-update) | async-done | bytes 524304 | tf_op jit(solution)/shard_map/psum | solution.py:68
  258.6 1.9 copy.118
  (32 shorter events, 0.3 us)
Async XLA Ops:
  7.2 89.1 %copy-start = (bf16[1,512,2048]{2,1,0:T(8,128)(2,1)S(1)}, bf16[1,512,2048]{2,1,0:T(8,128)(2,1)}, u32[]{:S(2)}) copy-start(bf16[1,512,2048]{2,1,0:T(8,128)(2,1)} %param.27) | copy-start | bytes 6291460
  7.2 82.5 %all-gather.4.cloned.1.call-start = ((), (), s32[]{:S(2)}) async-start(), calls=%async_computation.4 | async-start | bytes 5242880 | tf_op jit(solution)/shard_map/all_gather | solution.py:98
  56.0 95.3 %reduce-scatter.2.cloned.1.call-start = ((), (), s32[]{:S(2)}) async-start(), calls=%async_computation.5 | async-start | bytes 5242880 | tf_op jit(solution)/shard_map/reduce_scatter | solution.py:112
  106.6 115.8 %all-gather.6.cloned.1.call-start = ((), (), s32[]{:S(2)}) async-start(), calls=%async_computation.6 | async-start | bytes 5242880 | tf_op jit(solution)/shard_map/all_gather | solution.py:131
  158.1 31.4 %copy-start.1 = (bf16[128,2048]{1,0:T(8,128)(2,1)S(1)}, bf16[128,2048]{1,0:T(8,128)(2,1)}, u32[]{:S(2)}) copy-start(bf16[128,2048]{1,0:T(8,128)(2,1)} %param.14) | copy-start | bytes 1572868
  158.4 31.6 %copy-start.6 = (f32[2048]{0:T(1024)S(1)}, f32[2048]{0:T(1024)}, u32[]{:S(2)}) copy-start(f32[2048]{0:T(1024)} %param.15) | copy-start | bytes 24580
  189.5 69.1 %all-reduce.4.cloned.1.call-start = ((), (), s32[]{:S(2)}) async-start(), calls=%async_computation.3 | async-start | bytes 1048576 | tf_op jit(solution)/shard_map/psum | solution.py:68
  189.5 2.4 copy-start.5
  191.9 4.2 %copy-start.4 = (f32[128,4]{0,1:T(4,128)S(1)}, f32[128,4]{0,1:T(4,128)}, u32[]{:S(2)}) copy-start(f32[128,4]{0,1:T(4,128)} %param.24) | copy-start | bytes 6148
  191.9 4.2 %copy-start.2 = (f32[31,384]{1,0:T(8,128)S(1)}, f32[31,384]{1,0:T(8,128)}, u32[]{:S(2)}) copy-start(f32[31,384]{1,0:T(8,128)} %param.18) | copy-start | bytes 142852
  191.9 4.4 %copy-start.3 = (s32[128,4]{0,1:T(4,128)S(1)}, s32[128,4]{0,1:T(4,128)}, u32[]{:S(2)}) copy-start(s32[128,4]{0,1:T(4,128)} %param.23) | copy-start | bytes 6148
  192.0 12.9 %copy-start.7 = (f32[384]{0:T(512)S(1)}, f32[384]{0:T(512)}, u32[]{:S(2)}) copy-start(f32[384]{0:T(512)} %param.19) | copy-start | bytes 4612
  192.5 4.9 %collective-permute-start = (bf16[30,384]{1,0:T(8,128)(2,1)S(1)}, bf16[30,384]{1,0:T(8,128)(2,1)S(1)}, u32[]{:S(2)}, u32[]{:S(2)}) collective-permute-start(bf16[30,384]{1,0:T(8,128)(2,1)S(1)} %slice.260), channel_id=1, source_target_pairs={{0,4},{4,8},{8,12},{12,16},{16,20},{20,24},{24,28},{1,5},{5,9},{9,... | collective-permute-start | bytes 69128 | tf_op jit(solution)/shard_map/ppermute | solution.py:17
Sparse Core Ops, SparseCore 0:
  56.1 33.4 all-gather.3
  106.7 44.5 reduce-scatter.1
  189.6 32.7 all-gather.5
  225.1 33.4 all-reduce.3
